TPU v7x, 512 devices: a whole 4x8x8 slice. The times are simulated.
512 devices in a mesh: kv: 64 (over z, y), tp: 8 (over x, core).
Axes of the slice: x: 4, y: 8, z: 8, core: 2. Of those that a mesh axis runs over, the one named last changes fastest.
Arguments:
- queries: bfloat16 [8192, 1024], P('kv', 'tp'), may hold values from -4 to 4
- keys: bfloat16 [8192, 1024], P('kv', 'tp'), may hold values from -4 to 4
- values: bfloat16 [8192, 1024], P('kv', 'tp'), may hold values from -4 to 4
- cotangent: bfloat16 [8192, 1024], P('kv', 'tp'), may hold values from -4 to 4
- log_sum: float32 [16, 8192], P('tp', 'kv'), may hold values from 4.5 to 7.5
- chosen: int32 [16, 256, 12], P('tp'), may hold values from 0 to 255, as said below
- normed_input: bfloat16 [8192, 2048], P('kv', 'tp'), may hold values from -0.0625 to 0.0625
Outputs:
- grad_queries: bfloat16 [8192, 1024], P('kv', 'tp')
- grad_keys: bfloat16 [8192, 1024], P('kv', 'tp')
- grad_values: bfloat16 [8192, 1024], P('kv', 'tp')
- grad_weight: float32 [2048, 1024], P('kv', 'tp')
Inputs may be any that keep to these rules, and one draw needn't show every extreme that they name: `chosen`: for each head, the distinct blocks below their own query block that the query blocks of one device's 128 positions choose include at most 1 block of any one device's span of 128 positions, and exactly 1 for some pairs of devices. Within one list the entries below the query block's own index are distinct.
All inputs are finite; a program needn't handle non-finite values.
Results may differ from a plain program's by a relative error of at most 0.0085.
Values may be sent and summed in bfloat16 or wider, within the bound.
A program may use at most 64 MiB of HBM per device.

v0:
```python
import jax
import jax.numpy as jnp
from jax import lax
from jax.sharding import PartitionSpec as P

HD = 64
BLK = 32
SEL = 12
MOST = 1
MASKED = -1e30


def sent_together(arrays, axis, split_dim, concat_dim, along):
    both = jnp.concatenate(arrays, axis=along)
    whole, at, finished = (
        lax.all_to_all(both, axis, split_axis=split_dim, concat_axis=concat_dim, tiled=True),
        0,
        [],
    )
    for a in arrays:
        finished.append(lax.slice_in_dim(whole, at, at + a.shape[along], axis=along))
        at += a.shape[along]
    return tuple(finished)


def split_up(array, dim, size):
    dims = array.shape
    tiles = array.reshape(*dims[:dim], size, dims[dim] // size, *dims[dim + 1 :])
    return jnp.moveaxis(tiles, dim, 0)


def sum_at_owner(array, axis, dim):
    tiles = split_up(array, dim, lax.axis_size(axis))
    arrived = lax.all_to_all(tiles, axis, split_axis=0, concat_axis=0, tiled=True)
    return arrived.astype(jnp.float32).sum(axis=0)


def slot_picks(needed):
    span_width = needed.shape[-1]
    counted = needed.astype(jnp.int32)
    before = jnp.cumsum(counted, axis=-1) - counted
    places = jnp.arange(span_width, dtype=jnp.int32)
    picked, present = ([], [])
    hitting = needed & (before == 0)
    present.append(jnp.any(hitting, axis=-1))
    picked.append(jnp.sum(jnp.where(hitting, places, 0), axis=-1))
    return (jnp.stack(picked, axis=-1), jnp.stack(present, axis=-1))


def to_blocks(row_block, tok_rows, head_count):
    shards = row_block.shape[0] // tok_rows
    shaped = row_block.reshape(shards, tok_rows // BLK, BLK, head_count, HD).transpose(
        0, 3, 1, 2, 4
    )
    return shaped.reshape(shards * head_count * (tok_rows // BLK), BLK * HD)


def heads_from(row_block, head_count):
    blocks_dev = row_block.shape[0] // BLK
    return row_block.reshape(blocks_dev, BLK, head_count, HD).transpose(2, 0, 1, 3)


def back_rows(blocked):
    head_count, blocks_dev = (blocked.shape[0], blocked.shape[1])
    return blocked.transpose(1, 2, 0, 3).reshape(blocks_dev * BLK, head_count * HD)


def body(queries, keys, values, cotangent, log_sum, chosen, normed_input):
    tok_rows = queries.shape[0]
    head_count = log_sum.shape[0]
    blocks_dev = tok_rows // BLK
    devices = lax.axis_size("kv")
    my_index = lax.axis_index("kv")
    block_total = chosen.shape[1]
    tile_size = BLK * HD
    score_scale = HD ** (-0.5)
    places = jnp.arange(blocks_dev, dtype=jnp.int32)
    own_ids = my_index * blocks_dev + places
    my_lists = lax.dynamic_slice_in_dim(chosen, my_index * blocks_dev, blocks_dev, 1)
    usable = my_lists < own_ids[None, :, None]
    every_block = jnp.arange(block_total, dtype=jnp.int32)
    need_here = jnp.any((my_lists[..., None] == every_block) & usable[..., None], axis=(1, 2))
    req_picked, req_present = slot_picks(need_here.reshape(head_count, devices, blocks_dev))
    grouped = chosen.reshape(head_count, devices, blocks_dev, SEL)
    row_ids = every_block.reshape(devices, blocks_dev)
    usable_all = grouped < row_ids[None, :, :, None]
    need_there = jnp.any((grouped[..., None] == own_ids) & usable_all[..., None], axis=(2, 3))
    own_picked, own_present = slot_picks(need_there)
    own_picked = own_picked.transpose(1, 0, 2)
    own_present = own_present.transpose(1, 0, 2)
    head_base = (jnp.arange(head_count, dtype=jnp.int32) * blocks_dev)[None, :, None]
    send_ids = (head_base + own_picked).reshape(-1)
    key_send = jnp.take(to_blocks(keys, tok_rows, head_count), send_ids, axis=0).reshape(
        devices, head_count, MOST, tile_size
    )
    value_send = jnp.take(to_blocks(values, tok_rows, head_count), send_ids, axis=0).reshape(
        devices, head_count, MOST, tile_size
    )
    key_tiles, value_tiles = sent_together((key_send, value_send), "kv", 0, 0, 1)
    owners = my_lists // blocks_dev
    local_ids = my_lists % blocks_dev
    head_ids = jnp.arange(head_count, dtype=jnp.int32)[:, None, None]
    rows_at = (head_ids * devices + owners).reshape(-1)
    slot_at = jnp.take(req_picked.reshape(head_count * devices, MOST), rows_at, axis=0).reshape(
        head_count, blocks_dev, SEL, MOST
    )
    slot_live = jnp.take(req_present.reshape(head_count * devices, MOST), rows_at, axis=0).reshape(
        head_count, blocks_dev, SEL, MOST
    )
    matches = (slot_at == local_ids[..., None]) & slot_live
    slot_of = jnp.sum(jnp.where(matches, jnp.arange(MOST, dtype=jnp.int32), 0), axis=-1)
    tile_ids = jnp.where(usable, (owners * head_count + head_ids) * MOST + slot_of, 0).reshape(-1)
    sel_keys = jnp.take(key_tiles.reshape(-1, tile_size), tile_ids, axis=0).reshape(
        head_count, blocks_dev, SEL * BLK, HD
    )
    sel_values = jnp.take(value_tiles.reshape(-1, tile_size), tile_ids, axis=0).reshape(
        head_count, blocks_dev, SEL * BLK, HD
    )
    keys_all = jnp.concatenate([sel_keys, heads_from(keys, head_count)], axis=2)
    values_all = jnp.concatenate([sel_values, heads_from(values, head_count)], axis=2)
    causal = jnp.arange(BLK)[:, None] >= jnp.arange(BLK)[None, :]
    sel_mask = jnp.broadcast_to(
        jnp.repeat(usable, BLK, axis=2)[:, :, None, :], (head_count, blocks_dev, BLK, SEL * BLK)
    )
    allowed = jnp.concatenate(
        [sel_mask, jnp.broadcast_to(causal, (head_count, blocks_dev, BLK, BLK))], axis=3
    )
    q_blocks = heads_from(queries, head_count)
    g_blocks = heads_from(cotangent, head_count)
    log_rows = log_sum.reshape(head_count, blocks_dev, BLK)[..., None]
    scores = (
        jnp.einsum("hiqd,hikd->hiqk", q_blocks, keys_all, preferred_element_type=jnp.float32)
        * score_scale
    )
    weights = jnp.exp(jnp.where(allowed, scores - log_rows, MASKED))
    value_dots = jnp.einsum(
        "hiqd,hikd->hiqk", g_blocks, values_all, preferred_element_type=jnp.float32
    )
    row_delta = jnp.sum(weights * value_dots, axis=-1, keepdims=True)
    score_grad = (weights * (value_dots - row_delta)).astype(jnp.bfloat16)
    weights_low = weights.astype(jnp.bfloat16)
    query_grad = (
        jnp.einsum("hiqk,hikd->hiqd", score_grad, keys_all, preferred_element_type=jnp.float32)
        * score_scale
    )
    key_grad = (
        jnp.einsum("hiqk,hiqd->hikd", score_grad, q_blocks, preferred_element_type=jnp.float32)
        * score_scale
    )
    value_grad = jnp.einsum(
        "hiqk,hiqd->hikd", weights_low, g_blocks, preferred_element_type=jnp.float32
    )
    grad_queries = back_rows(query_grad).astype(jnp.bfloat16)

    def to_slots(gradient):
        chosen_part = gradient[:, :, : SEL * BLK].reshape(-1, tile_size)
        slotted = jax.ops.segment_sum(
            chosen_part, tile_ids, num_segments=devices * head_count * MOST
        )
        return slotted.reshape(devices, head_count, MOST, tile_size)

    back_keys, back_values = (
        lax.all_to_all(
            to_slots(key_grad).astype(jnp.bfloat16), "kv", split_axis=0, concat_axis=0, tiled=True
        ).astype(jnp.float32),
        lax.all_to_all(
            to_slots(value_grad).astype(jnp.bfloat16), "kv", split_axis=0, concat_axis=0, tiled=True
        ).astype(jnp.float32),
    )
    land_ids = jnp.where(own_present, head_base + own_picked, head_count * blocks_dev).reshape(-1)

    def settle(returned, gradient):
        flat_tiles = returned.reshape(-1, tile_size)
        targets = (
            jnp.arange(head_count * blocks_dev, dtype=jnp.int32)[:, None] == land_ids[None, :]
        ).astype(jnp.float32)
        landed = jnp.dot(
            targets, flat_tiles, precision=lax.Precision.HIGHEST, preferred_element_type=jnp.float32
        )
        summed = landed.reshape(head_count, blocks_dev, BLK, HD) + gradient[:, :, SEL * BLK :]
        return back_rows(summed).astype(jnp.bfloat16)

    grad_keys = settle(back_keys, key_grad)
    grad_values = settle(back_values, value_grad)
    whole_input = lax.all_gather(normed_input, "tp", axis=1, tiled=True)
    grad_weight = sum_at_owner(
        lax.dot_general(
            whole_input, grad_queries, (((0,), (0,)), ((), ())), preferred_element_type=jnp.float32
        ).astype(jnp.bfloat16),
        "kv",
        0,
    )
    return (grad_queries, grad_keys, grad_values, grad_weight)


def solution(mesh):
    in_specs = (
        P("kv", "tp"),
        P("kv", "tp"),
        P("kv", "tp"),
        P("kv", "tp"),
        P("tp", "kv"),
        P("tp", None, None),
        P("kv", "tp"),
    )
    out_specs = (P("kv", "tp"), P("kv", "tp"), P("kv", "tp"), P("kv", "tp"))
    return jax.shard_map(body, mesh=mesh, in_specs=in_specs, out_specs=out_specs, check_vma=False)
```

profile of v0, /device:TPU:8, one launch (start us, length us, event | category | flops | bytes accessed | tf_op | source)
XLA Modules:
  0.0 145.6 jit_solution(14934738471255190425)
XLA Ops:
  0.7 0.9 copy.75
  2.6 0.8 reshape.213
  3.9 0.9 gather_fusion
  4.8 0.9 gather_fusion.1
  6.0 0.3 reshape.219
  6.3 0.3 reshape.216
  6.6 2.1 %pad_maximum_fusion = bf16[64,4,1,2048]{3,1,2,0:T(4,128)(2,1)} fusion(bf16[64,2,1,2048]{3,1,2,0:T(2,128)(2,1)S(1)} %bitcast.101, bf16[64,2,1,2048]{3,1,2,0:T(2,128)(2,1)S(1)} %bitcast.102), kind=kLoop, calls=%fused_computation.18 | loop fusion | flops 2097152 | bytes 2097152 | tf_op jit(solution)/shard_map/concatenate | solution.py:14
  8.7 16.7 %all-to-all-start = ((bf16[64,4,1,2048]{3,1,2,0:T(4,128)(2,1)}), bf16[64,4,1,2048]{3,1,2,0:T(4,128)(2,1)S(1)}, u32[]{:S(2)}, u32[]{:S(2)}) async-start(bf16[64,4,1,2048]{3,1,2,0:T(4,128)(2,1)} %pad_maximum_fusion), calls=%async_computation | async-start | bytes 2097152 | tf_op jit(solution)/shard_map/all_to_all | solution.py:16
  26.9 27.8 %all-to-all-done = bf16[64,4,1,2048]{3,1,2,0:T(4,128)(2,1)S(1)} async-done(((bf16[64,4,1,2048]{3,1,2,0:T(4,128)(2,1)}), bf16[64,4,1,2048]{3,1,2,0:T(4,128)(2,1)S(1)}, u32[]{:S(2)}, u32[]{:S(2)}) %all-to-all-start) | async-done | bytes 1048608 | tf_op jit(solution)/shard_map/all_to_all | solution.py:16
  54.7 0.7 fusion.46
  55.9 0.8 gather_fusion.3
  56.7 0.8 gather_fusion.2
  57.7 0.8 reshape.226
  58.5 0.3 copy.87
  58.8 0.8 reshape.222
  59.6 0.3 copy.84
  60.2 0.4 multiply_reduce_fusion
  60.8 0.3 convolution_multiply_fusion
  61.2 0.3 copy-done.1
  61.7 0.5 copy.91
  62.1 0.5 reshape.270
  62.6 2.0 %scatter_custom_fusion = f32[128,2048]{1,0:T(8,128)S(1)} fusion(s32[96]{0:T(128)S(1)} %reshape.221, f32[96,2048]{1,0:T(8,128)S(1)} %reshape.270, f32[]{:T(128)} %constant.105.clone.1), kind=kCustom, calls=%fused_computation.26 | custom fusion | flops 196608 | bytes 1048580 | tf_op jit(solution)/shard_map/scatter-add | solution.py:157
  64.7 1.2 convert_element_type.84
  65.9 7.1 %all-to-all-start.1 = ((bf16[64,2,1,2048]{3,1,2,0:T(2,128)(2,1)}), bf16[64,2,1,2048]{3,1,2,0:T(2,128)(2,1)}, u32[]{:S(2)}, u32[]{:S(2)}) async-start(bf16[64,2,1,2048]{3,1,2,0:T(2,128)(2,1)} %bitcast.18), calls=%async_computation.1 | async-start | bytes 1048576 | tf_op jit(solution)/shard_map/all_to_all | solution.py:163
  73.1 0.3 fusion.16
  73.4 1.0 copy-done
  74.4 0.5 copy.96
  74.9 0.5 reshape.278
  75.4 2.0 %scatter_custom_fusion.1 = f32[128,2048]{1,0:T(8,128)S(1)} fusion(s32[96]{0:T(128)S(1)} %reshape.221, f32[96,2048]{1,0:T(8,128)S(1)} %reshape.278, f32[]{:T(128)} %constant.105.clone.1), kind=kCustom, calls=%fused_computation.24 | custom fusion | flops 196608 | bytes 1048580 | tf_op jit(solution)/shard_map/scatter-add | solution.py:157
  77.6 1.1 convert_element_type.90
  78.7 12.8 %all-to-all-done.1 = bf16[64,2,1,2048]{3,1,2,0:T(2,128)(2,1)} async-done(((bf16[64,2,1,2048]{3,1,2,0:T(2,128)(2,1)}), bf16[64,2,1,2048]{3,1,2,0:T(2,128)(2,1)}, u32[]{:S(2)}, u32[]{:S(2)}) %all-to-all-start.1) | async-done | bytes 524320 | tf_op jit(solution)/shard_map/all_to_all | solution.py:163
  91.5 5.4 %all-to-all-start.2 = ((bf16[64,2,1,2048]{3,1,2,0:T(2,128)(2,1)}), bf16[64,2,1,2048]{3,1,2,0:T(2,128)(2,1)S(1)}, u32[]{:S(2)}, u32[]{:S(2)}) async-start(bf16[64,2,1,2048]{3,1,2,0:T(2,128)(2,1)} %bitcast.24), calls=%async_computation.2 | async-start | bytes 1048576 | tf_op jit(solution)/shard_map/all_to_all | solution.py:166
  97.2 13.5 %all_gather.3 = bf16[128,2048]{1,0:T(8,128)(2,1)S(1)} all-gather(bf16[128,256]{1,0:T(8,128)(2,1)S(1)} %copy-done.12), channel_id=1, replica_groups=mesh['kv'=64,'tp'=8] {'tp'}, dimensions={1}, use_global_device_ids=true | all-gather | bytes 589824 | tf_op jit(solution)/shard_map/all_gather | solution.py:185
  110.6 0.3 fusion.6
  111.1 0.3 fusion
  111.4 1.0 copy.101
  112.4 2.6 %all-to-all-done.2 = bf16[64,2,1,2048]{3,1,2,0:T(2,128)(2,1)S(1)} async-done(((bf16[64,2,1,2048]{3,1,2,0:T(2,128)(2,1)}), bf16[64,2,1,2048]{3,1,2,0:T(2,128)(2,1)S(1)}, u32[]{:S(2)}, u32[]{:S(2)}) %all-to-all-start.2) | async-done | bytes 524320 | tf_op jit(solution)/shard_map/all_to_all | solution.py:166
  115.0 10.1 %all-to-all-start.3 = ((bf16[64,32,128]{2,1,0:T(8,128)(2,1)}), bf16[64,32,128]{2,1,0:T(8,128)(2,1)S(1)}, u32[]{:S(2)}, u32[]{:S(2)}) async-start(bf16[64,32,128]{2,1,0:T(8,128)(2,1)} %bitcast.30), calls=%async_computation.3 | async-start | bytes 1048576 | tf_op jit(solution)/shard_map/all_to_all | solution.py:34
  125.2 1.2 reshape.230
  126.4 0.3 copy.93
  126.7 0.5 fusion.31
  127.6 0.7 convert_element_type.87
  128.5 0.3 copy.98
  128.7 0.5 fusion.29
  129.4 1.0 fusion.19
  130.5 0.7 convert_element_type.93
  131.3 13.6 %all-to-all-done.3 = bf16[64,32,128]{2,1,0:T(8,128)(2,1)S(1)} async-done(((bf16[64,32,128]{2,1,0:T(8,128)(2,1)}), bf16[64,32,128]{2,1,0:T(8,128)(2,1)S(1)}, u32[]{:S(2)}, u32[]{:S(2)}) %all-to-all-start.3) | async-done | bytes 524320 | tf_op jit(solution)/shard_map/all_to_all | solution.py:34
  144.9 0.7 convert_reduce_fusion
  (94 shorter events, 5.5 us)
Async XLA Ops:
  0.6 3.0 %copy-start.7 = (bf16[128,128]{1,0:T(8,128)(2,1)S(1)}, bf16[128,128]{1,0:T(8,128)(2,1)}, u32[]{:S(2)}) copy-start(bf16[128,128]{1,0:T(8,128)(2,1)} %param.13) | copy-start | bytes 98308
  8.7 16.9 %copy-start.8 = (bf16[128,128]{1,0:T(8,128)(2,1)S(1)}, bf16[128,128]{1,0:T(8,128)(2,1)}, u32[]{:S(2)}) copy-start(bf16[128,128]{1,0:T(8,128)(2,1)} %param.12) | copy-start | bytes 98308
  8.7 17.1 %copy-start.13 = (s32[2,256,12]{1,0,2:T(2,128)S(1)}, s32[2,256,12]{1,0,2:T(2,128)}, u32[]{:S(2)}) copy-start(s32[2,256,12]{1,0,2:T(2,128)} %param.16) | copy-start | bytes 73732
  8.7 17.4 %copy-start.14 = (bf16[128,128]{1,0:T(8,128)(2,1)S(1)}, bf16[128,128]{1,0:T(8,128)(2,1)}, u32[]{:S(2)}) copy-start(bf16[128,128]{1,0:T(8,128)(2,1)} %param.14) | copy-start | bytes 98308
  8.7 17.5 %copy-start.16 = (f32[2,128]{1,0:T(2,128)S(1)}, f32[2,128]{1,0:T(2,128)}, u32[]{:S(2)}) copy-start(f32[2,128]{1,0:T(2,128)} %param.15) | copy-start | bytes 3076
  8.7 17.7 %copy-start.15 = (bf16[128,128]{1,0:T(8,128)(2,1)S(1)}, bf16[128,128]{1,0:T(8,128)(2,1)}, u32[]{:S(2)}) copy-start(bf16[128,128]{1,0:T(8,128)(2,1)} %param.11) | copy-start | bytes 98308
  8.7 46.0 %all-to-all-start = ((bf16[64,4,1,2048]{3,1,2,0:T(4,128)(2,1)}), bf16[64,4,1,2048]{3,1,2,0:T(4,128)(2,1)S(1)}, u32[]{:S(2)}, u32[]{:S(2)}) async-start(bf16[64,4,1,2048]{3,1,2,0:T(4,128)(2,1)} %pad_maximum_fusion), calls=%async_computation | async-start | bytes 2097152 | tf_op jit(solution)/shard_map/all_to_all | solution.py:16
  26.4 33.8 %copy-start.10 = (bf16[4,32,2,64]{1,3,0,2:T(8,128)(2,1)}, bf16[4,32,2,64]{1,3,0,2:T(8,128)(2,1)S(1)}, u32[]{:S(2)}) copy-start(bf16[4,32,2,64]{1,3,0,2:T(8,128)(2,1)S(1)} %copy.83) | copy-start | bytes 98308
  59.9 0.8 copy-start.5
  60.7 0.8 copy-start.1
  60.8 0.8 copy-start.3
  64.7 8.4 %copy-start.2 = (f32[2,4,32,416]{3,2,1,0:T(8,128)S(1)}, f32[2,4,32,416]{3,2,1,0:T(8,128)}, u32[]{:S(2)}) copy-start(f32[2,4,32,416]{3,2,1,0:T(8,128)} %copy-done.1) | copy-start | bytes 1277956
  65.9 25.6 %all-to-all-start.1 = ((bf16[64,2,1,2048]{3,1,2,0:T(2,128)(2,1)}), bf16[64,2,1,2048]{3,1,2,0:T(2,128)(2,1)}, u32[]{:S(2)}, u32[]{:S(2)}) async-start(bf16[64,2,1,2048]{3,1,2,0:T(2,128)(2,1)} %bitcast.18), calls=%async_computation.1 | async-start | bytes 1048576 | tf_op jit(solution)/shard_map/all_to_all | solution.py:163
  73.4 1.0 copy-start
  77.4 19.7 %copy-start.12 = (bf16[128,256]{1,0:T(8,128)(2,1)S(1)}, bf16[128,256]{1,0:T(8,128)(2,1)}, u32[]{:S(2)}) copy-start(bf16[128,256]{1,0:T(8,128)(2,1)} %param.17) | copy-start | bytes 196612
  77.5 33.1 %copy-start.4 = (bf16[2,4,32,416]{3,2,1,0:T(8,128)(2,1)S(1)}, bf16[2,4,32,416]{3,2,1,0:T(8,128)(2,1)}, u32[]{:S(2)}) copy-start(bf16[2,4,32,416]{3,2,1,0:T(8,128)(2,1)} %copy-done.3) | copy-start | bytes 638980
  77.5 33.1 %copy-start.6 = (bf16[2,4,384,64]{2,3,1,0:T(8,128)(2,1)S(1)}, bf16[2,4,384,64]{2,3,1,0:T(8,128)(2,1)}, u32[]{:S(2)}) copy-start(bf16[2,4,384,64]{2,3,1,0:T(8,128)(2,1)} %copy-done.5) | copy-start | bytes 1179652
  77.5 33.1 %copy-start.11 = (bf16[4,32,2,64]{1,3,0,2:T(8,128)(2,1)S(1)}, bf16[4,32,2,64]{1,3,0,2:T(8,128)(2,1)}, u32[]{:S(2)}) copy-start(bf16[4,32,2,64]{1,3,0,2:T(8,128)(2,1)} %copy-done.10) | copy-start | bytes 98308
  91.5 23.6 %all-to-all-start.2 = ((bf16[64,2,1,2048]{3,1,2,0:T(2,128)(2,1)}), bf16[64,2,1,2048]{3,1,2,0:T(2,128)(2,1)S(1)}, u32[]{:S(2)}, u32[]{:S(2)}) async-start(bf16[64,2,1,2048]{3,1,2,0:T(2,128)(2,1)} %bitcast.24), calls=%async_computation.2 | async-start | bytes 1048576 | tf_op jit(solution)/shard_map/all_to_all | solution.py:166
  111.1 3.9 %copy-start.9 = (bf16[128,128]{1,0:T(8,128)(2,1)}, bf16[128,128]{1,0:T(8,128)(2,1)S(1)}, u32[]{:S(2)}) copy-start(bf16[128,128]{1,0:T(8,128)(2,1)S(1)} %convert_element_type.82) | copy-start | bytes 98308
  115.0 29.8 %all-to-all-start.3 = ((bf16[64,32,128]{2,1,0:T(8,128)(2,1)}), bf16[64,32,128]{2,1,0:T(8,128)(2,1)S(1)}, u32[]{:S(2)}, u32[]{:S(2)}) async-start(bf16[64,32,128]{2,1,0:T(8,128)(2,1)} %bitcast.30), calls=%async_computation.3 | async-start | bytes 1048576 | tf_op jit(solution)/shard_map/all_to_all | solution.py:34
where the time goes:
time: 146 us
  waiting for transfers between devices  56.8 us (39%)
  starting transfers between devices  39.4 us (27%)
  local copies, waits for them, and re-layouts  22.7 us (16%)
  blocking collectives  13.5 us (9%)
  other arithmetic  8.99 us (6%)
  matrix products  2.89 us (2%)
    all_to_all x1, waiting for transfers between devices, sent_together(): lax.all_to_all(both, axis, split_axis=split_dim, concat_axis=concat_dim,...  27.8 us
    all_to_all x1, starting transfers between devices, sent_together(): lax.all_to_all(both, axis, split_axis=split_dim, concat_axis=concat_dim,...  16.7 us
    all_to_all x1, waiting for transfers between devices, sum_at_owner(): lax.all_to_all(tiles, axis, split_axis=0, concat_axis=0, tiled=True)  13.6 us
    all_gather x1, blocking collectives, body(): whole_input = lax.all_gather(normed_input, 'tp', axis=1, tiled=True)  13.5 us
    all_to_all x1, waiting for transfers between devices, body(): lax.all_to_all(to_slots(key_grad).astype(jnp.bfloat16), 'kv', split_axis=...  12.8 us
    all_to_all x1, starting transfers between devices, sum_at_owner(): lax.all_to_all(tiles, axis, split_axis=0, concat_axis=0, tiled=True)  10.1 us
    all_to_all x1, starting transfers between devices, body(): lax.all_to_all(to_slots(key_grad).astype(jnp.bfloat16), 'kv', split_axis=...  7.14 us
    all_to_all x1, starting transfers between devices, body(): lax.all_to_all(to_slots(value_grad).astype(jnp.bfloat16), 'kv', split_axi...  5.45 us
  transfers between devices with their start and end apart: 4, of which 4 were waited for; matrix products, arithmetic and copies ran while one was open for 10% of the time, Pallas kernels for 0%

commit v1 on v0

--- a/solution.py
+++ b/solution.py
@@ -8,6 +8,13 @@
 SEL = 12
 MOST = 1
 MASKED = -1e30
+
+
+def do_packet(target, array_axis):
+    side_arr = list(target.shape[1:])
+    side_arr[array_axis] *= target.shape[0]
+    e_now = jnp.moveaxis(target, 0, array_axis).reshape(side_arr)
+    return e_now
 
 
 def sent_together(arrays, axis, split_dim, concat_dim, along):
@@ -182,7 +189,36 @@
 
     grad_keys = settle(back_keys, key_grad)
     grad_values = settle(back_values, value_grad)
-    whole_input = lax.all_gather(normed_input, "tp", axis=1, tiled=True)
+    buffer = []
+    no = 0
+    ndev = lax.axis_size("tp")
+    while no < ndev:
+        buffer.append((no, (no + 1) % ndev))
+        no += 1
+    frames = []
+    for m, q in buffer:
+        frames.append((q, m))
+    view_out, left_arr = ([], [])
+    i0 = 0
+    while i0 < ndev - 1:
+        if i0 % 2 == 0:
+            view_out.append(
+                lax.ppermute(
+                    view_out[-1] if view_out else normed_input, perm=buffer, axis_name="tp"
+                )
+            )
+        else:
+            frame_out = lax.ppermute(
+                left_arr[-1] if left_arr else normed_input, perm=frames, axis_name="tp"
+            )
+            left_arr.append(frame_out)
+        i0 += 1
+    n_now = jnp.stack([*view_out[::-1], normed_input, *left_arr], axis=0)
+    u1 = len(view_out)
+    outer = lax.axis_index("tp")
+    opened = outer - u1
+    n_now = n_now[(jnp.arange(ndev) - opened) % ndev]
+    whole_input = do_packet(n_now, 1)
     grad_weight = sum_at_owner(
         lax.dot_general(
             whole_input, grad_queries, (((0,), (0,)), ((), ())), preferred_element_type=jnp.float32

time: 146 us -> 141 us (0.966)
  the two profiles are of different devices: /device:TPU:8 before, /device:TPU:6 now
where the time goes in v1:
time: 141 us; the launch traced here: 140 us
  waiting for transfers between devices  57.8 us (41%)
  starting transfers between devices  39.6 us (28%)
  local copies, waits for them, and re-layouts  27.3 us (19%)
  other arithmetic  9.05 us (6%)
  matrix products  4.65 us (3%)
  between operations  1.45 us (1%)
    all_to_all x1, starting transfers between devices, sent_together(): lax.all_to_all(both, axis, split_axis=split_dim, concat_axis=concat_dim,...  16.9 us
    all_to_all x1, waiting for transfers between devices, sent_together(): lax.all_to_all(both, axis, split_axis=split_dim, concat_axis=concat_dim,...  14.1 us
    all_to_all x1, waiting for transfers between devices, body(): lax.all_to_all(to_slots(value_grad).astype(jnp.bfloat16), 'kv', split_axi...  13.3 us
    all_to_all x1, waiting for transfers between devices, sum_at_owner(): lax.all_to_all(tiles, axis, split_axis=0, concat_axis=0, tiled=True)  12.1 us
    all_to_all x1, waiting for transfers between devices, body(): lax.all_to_all(to_slots(key_grad).astype(jnp.bfloat16), 'kv', split_axis=...  10.4 us
    ppermute x4, waiting for transfers between devices, body(): lax.ppermute(view_out[-1] if view_out else normed_input, perm=buffer, axi...  7.8 us
    all_to_all x1, starting transfers between devices, body(): lax.all_to_all(to_slots(key_grad).astype(jnp.bfloat16), 'kv', split_axis=...  6.75 us
    unnamed x58, local copies, waits for them, and re-layouts  6.36 us
  transfers between devices with their start and end apart: 11, of which 8 were waited for; matrix products, arithmetic and copies ran while one was open for 22% of the time, Pallas kernels for 0%

profile of v1, /device:TPU:6, one launch (start us, length us, event | category | flops | bytes accessed | tf_op | source)
XLA Modules:
  0.0 139.8 jit_solution(4081483890278886516)
XLA Ops:
  0.7 0.9 copy.97
  2.7 0.8 reshape.266
  4.3 0.9 gather_fusion.1
  5.2 0.9 gather_fusion.2
  7.0 2.1 %pad_maximum_fusion = bf16[64,4,1,2048]{3,1,2,0:T(4,128)(2,1)} fusion(bf16[64,2,1,2048]{3,1,2,0:T(2,128)(2,1)S(1)} %bitcast.121, bf16[64,2,1,2048]{3,1,2,0:T(2,128)(2,1)S(1)} %bitcast.122), kind=kLoop, calls=%fused_computation.18 | loop fusion | flops 2097152 | bytes 2097152 | tf_op jit(solution)/shard_map/concatenate | solution.py:21
  9.1 16.9 %all-to-all-start = ((bf16[64,4,1,2048]{3,1,2,0:T(4,128)(2,1)}), bf16[64,4,1,2048]{3,1,2,0:T(4,128)(2,1)S(1)}, u32[]{:S(2)}, u32[]{:S(2)}) async-start(bf16[64,4,1,2048]{3,1,2,0:T(4,128)(2,1)} %pad_maximum_fusion), calls=%async_computation | async-start | bytes 2097152 | tf_op jit(solution)/shard_map/all_to_all | solution.py:23
  26.1 1.7 %collective-permute-start.4 = (bf16[128,256]{1,0:T(8,128)(2,1)S(1)}, bf16[128,256]{1,0:T(8,128)(2,1)S(1)}, u32[]{:S(2)}, u32[]{:S(2)}) collective-permute-start(bf16[128,256]{1,0:T(8,128)(2,1)S(1)} %copy-done.12), channel_id=1, source_target_pairs={{1,0},{2,1},{3,2},{4,3},{5,4},{6,5},{7,6},{0,7},{9,8},{10,9},{11,1... | collective-permute-start | bytes 196616 | tf_op jit(solution)/shard_map/ppermute | solution.py:211
  29.1 0.6 collective-permute-done
  29.7 3.7 %collective-permute-done.1 = bf16[128,256]{1,0:T(8,128)(2,1)S(1)} collective-permute-done((bf16[128,256]{1,0:T(8,128)(2,1)S(1)}, bf16[128,256]{1,0:T(8,128)(2,1)S(1)}, u32[]{:S(2)}, u32[]{:S(2)}) %collective-permute-start.1) | collective-permute-done | bytes 65568 | tf_op jit(solution)/shard_map/ppermute | solution.py:206
  33.5 1.8 %collective-permute-start.5 = (bf16[128,256]{1,0:T(8,128)(2,1)S(1)}, bf16[128,256]{1,0:T(8,128)(2,1)}, u32[]{:S(2)}, u32[]{:S(2)}) collective-permute-start(bf16[128,256]{1,0:T(8,128)(2,1)S(1)} %collective-permute-done.4), channel_id=1, source_target_pairs={{1,0},{2,1},{3,2},{4,3},{5,4},{6,5},{7,6},{0,7},{9,8},{10,9},{11,1... | collective-permute-start | bytes 196616 | tf_op jit(solution)/shard_map/ppermute | solution.py:211
  35.2 1.9 %collective-permute-done.2 = bf16[128,256]{1,0:T(8,128)(2,1)S(1)} collective-permute-done((bf16[128,256]{1,0:T(8,128)(2,1)S(1)}, bf16[128,256]{1,0:T(8,128)(2,1)S(1)}, u32[]{:S(2)}, u32[]{:S(2)}) %collective-permute-start.2) | collective-permute-done | bytes 65568 | tf_op jit(solution)/shard_map/ppermute | solution.py:206
  37.1 0.7 collective-permute-start.3
  37.8 1.4 %collective-permute-start.6 = (bf16[128,256]{1,0:T(8,128)(2,1)}, bf16[128,256]{1,0:T(8,128)(2,1)}, u32[]{:S(2)}, u32[]{:S(2)}) collective-permute-start(bf16[128,256]{1,0:T(8,128)(2,1)} %collective-permute-done.5), channel_id=1, source_target_pairs={{1,0},{2,1},{3,2},{4,3},{5,4},{6,5},{7,6},{0,7},{9,8},{10,9},{11,1... | collective-permute-start | bytes 196616 | tf_op jit(solution)/shard_map/ppermute | solution.py:211
  39.2 1.6 %collective-permute-done.3 = bf16[128,256]{1,0:T(8,128)(2,1)S(1)} collective-permute-done((bf16[128,256]{1,0:T(8,128)(2,1)S(1)}, bf16[128,256]{1,0:T(8,128)(2,1)S(1)}, u32[]{:S(2)}, u32[]{:S(2)}) %collective-permute-start.3) | collective-permute-done | bytes 65568 | tf_op jit(solution)/shard_map/ppermute | solution.py:206
  40.8 0.6 bitcast_dynamic-update-slice_fusion.7
  41.4 14.1 %all-to-all-done = bf16[64,4,1,2048]{3,1,2,0:T(4,128)(2,1)S(1)} async-done(((bf16[64,4,1,2048]{3,1,2,0:T(4,128)(2,1)}), bf16[64,4,1,2048]{3,1,2,0:T(4,128)(2,1)S(1)}, u32[]{:S(2)}, u32[]{:S(2)}) %all-to-all-start) | async-done | bytes 1048608 | tf_op jit(solution)/shard_map/all_to_all | solution.py:23
  55.6 0.7 fusion.47
  56.8 0.8 gather_fusion.4
  57.6 0.8 gather_fusion.3
  58.6 0.8 reshape.279
  59.7 0.8 reshape.275
  63.4 2.0 %scatter_custom_fusion = f32[128,2048]{1,0:T(8,128)S(1)} fusion(s32[96]{0:T(128)S(1)} %reshape.274, f32[96,2048]{1,0:T(8,128)S(1)} %reshape.332, f32[]{:T(128)} %constant.121.clone.1), kind=kCustom, calls=%fused_computation.26 | custom fusion | flops 196608 | bytes 1048580 | tf_op jit(solution)/shard_map/scatter-add | solution.py:164
  65.6 1.1 convert_element_type.83
  66.7 6.7 %all-to-all-start.1 = ((bf16[64,2,1,2048]{3,1,2,0:T(2,128)(2,1)}), bf16[64,2,1,2048]{3,1,2,0:T(2,128)(2,1)}, u32[]{:S(2)}, u32[]{:S(2)}) async-start(bf16[64,2,1,2048]{3,1,2,0:T(2,128)(2,1)} %bitcast.18), calls=%async_computation.1 | async-start | bytes 1048576 | tf_op jit(solution)/shard_map/all_to_all | solution.py:170
  73.5 0.6 bitcast_dynamic-update-slice_fusion.6
  74.1 0.6 bitcast_dynamic-update-slice_fusion.5
  74.7 0.6 bitcast_dynamic-update-slice_fusion.4
  75.4 0.6 bitcast_dynamic-update-slice_fusion.3
  76.4 1.0 copy-done
  78.4 2.0 %scatter_custom_fusion.1 = f32[128,2048]{1,0:T(8,128)S(1)} fusion(s32[96]{0:T(128)S(1)} %reshape.274, f32[96,2048]{1,0:T(8,128)S(1)} %reshape.340, f32[]{:T(128)} %constant.121.clone.1), kind=kCustom, calls=%fused_computation.24 | custom fusion | flops 196608 | bytes 1048580 | tf_op jit(solution)/shard_map/scatter-add | solution.py:164
  80.5 1.1 convert_element_type.89
  81.7 10.4 %all-to-all-done.1 = bf16[64,2,1,2048]{3,1,2,0:T(2,128)(2,1)} async-done(((bf16[64,2,1,2048]{3,1,2,0:T(2,128)(2,1)}), bf16[64,2,1,2048]{3,1,2,0:T(2,128)(2,1)}, u32[]{:S(2)}, u32[]{:S(2)}) %all-to-all-start.1) | async-done | bytes 524320 | tf_op jit(solution)/shard_map/all_to_all | solution.py:170
  92.1 5.3 %all-to-all-start.2 = ((bf16[64,2,1,2048]{3,1,2,0:T(2,128)(2,1)}), bf16[64,2,1,2048]{3,1,2,0:T(2,128)(2,1)S(1)}, u32[]{:S(2)}, u32[]{:S(2)}) async-start(bf16[64,2,1,2048]{3,1,2,0:T(2,128)(2,1)} %bitcast.24), calls=%async_computation.2 | async-start | bytes 1048576 | tf_op jit(solution)/shard_map/all_to_all | solution.py:173
  97.4 0.8 bitcast_dynamic-update-slice_fusion.1
  98.3 0.8 bitcast_dynamic-update-slice_fusion
  99.1 0.6 gather_fusion
  100.0 1.3 fusion.5
  101.5 1.1 convolution_convert_fusion
  102.5 13.3 %all-to-all-done.2 = bf16[64,2,1,2048]{3,1,2,0:T(2,128)(2,1)S(1)} async-done(((bf16[64,2,1,2048]{3,1,2,0:T(2,128)(2,1)}), bf16[64,2,1,2048]{3,1,2,0:T(2,128)(2,1)S(1)}, u32[]{:S(2)}, u32[]{:S(2)}) %all-to-all-start.2) | async-done | bytes 524320 | tf_op jit(solution)/shard_map/all_to_all | solution.py:173
  115.8 5.0 %all-to-all-start.3 = ((bf16[64,32,128]{2,1,0:T(8,128)(2,1)}), bf16[64,32,128]{2,1,0:T(8,128)(2,1)S(1)}, u32[]{:S(2)}, u32[]{:S(2)}) async-start(bf16[64,32,128]{2,1,0:T(8,128)(2,1)} %bitcast.40), calls=%async_computation.3 | async-start | bytes 1048576 | tf_op jit(solution)/shard_map/all_to_all | solution.py:41
  120.9 1.2 reshape.283
  122.4 0.5 fusion.30
  123.3 0.7 convert_element_type.86
  124.4 0.5 fusion.28
  125.1 1.0 fusion.18
  126.2 0.7 convert_element_type.92
  127.0 12.1 %all-to-all-done.3 = bf16[64,32,128]{2,1,0:T(8,128)(2,1)S(1)} async-done(((bf16[64,32,128]{2,1,0:T(8,128)(2,1)}), bf16[64,32,128]{2,1,0:T(8,128)(2,1)S(1)}, u32[]{:S(2)}, u32[]{:S(2)}) %all-to-all-start.3) | async-done | bytes 524320 | tf_op jit(solution)/shard_map/all_to_all | solution.py:41
  139.1 0.7 convert_reduce_fusion
  (133 shorter events, 10.9 us)
Async XLA Ops:
  0.6 3.0 %copy-start.21 = (s32[2,256,12]{1,0,2:T(2,128)S(1)}, s32[2,256,12]{1,0,2:T(2,128)}, u32[]{:S(2)}) copy-start(s32[2,256,12]{1,0,2:T(2,128)} %param.16) | copy-start | bytes 73732
  0.6 3.4 %copy-start.7 = (bf16[128,128]{1,0:T(8,128)(2,1)S(1)}, bf16[128,128]{1,0:T(8,128)(2,1)}, u32[]{:S(2)}) copy-start(bf16[128,128]{1,0:T(8,128)(2,1)} %param.13) | copy-start | bytes 98308
  9.1 16.9 %copy-start.12 = (bf16[128,256]{1,0:T(8,128)(2,1)S(1)}, bf16[128,256]{1,0:T(8,128)(2,1)}, u32[]{:S(2)}) copy-start(bf16[128,256]{1,0:T(8,128)(2,1)} %param.17) | copy-start | bytes 196612
  9.1 18.8 %copy-start.8 = (bf16[128,128]{1,0:T(8,128)(2,1)S(1)}, bf16[128,128]{1,0:T(8,128)(2,1)}, u32[]{:S(2)}) copy-start(bf16[128,128]{1,0:T(8,128)(2,1)} %param.12) | copy-start | bytes 98308
  9.1 19.0 %copy-start.22 = (bf16[128,128]{1,0:T(8,128)(2,1)S(1)}, bf16[128,128]{1,0:T(8,128)(2,1)}, u32[]{:S(2)}) copy-start(bf16[128,128]{1,0:T(8,128)(2,1)} %param.14) | copy-start | bytes 98308
  9.1 19.1 %copy-start.24 = (f32[2,128]{1,0:T(2,128)S(1)}, f32[2,128]{1,0:T(2,128)}, u32[]{:S(2)}) copy-start(f32[2,128]{1,0:T(2,128)} %param.15) | copy-start | bytes 3076
  9.1 19.4 %copy-start.23 = (bf16[128,128]{1,0:T(8,128)(2,1)S(1)}, bf16[128,128]{1,0:T(8,128)(2,1)}, u32[]{:S(2)}) copy-start(bf16[128,128]{1,0:T(8,128)(2,1)} %param.11) | copy-start | bytes 98308
  9.1 46.5 %all-to-all-start = ((bf16[64,4,1,2048]{3,1,2,0:T(4,128)(2,1)}), bf16[64,4,1,2048]{3,1,2,0:T(4,128)(2,1)S(1)}, u32[]{:S(2)}, u32[]{:S(2)}) async-start(bf16[64,4,1,2048]{3,1,2,0:T(4,128)(2,1)} %pad_maximum_fusion), calls=%async_computation | async-start | bytes 2097152 | tf_op jit(solution)/shard_map/all_to_all | solution.py:23
  26.0 3.7 %collective-permute-start = (bf16[128,256]{1,0:T(8,128)(2,1)S(1)}, bf16[128,256]{1,0:T(8,128)(2,1)S(1)}, u32[]{:S(2)}, u32[]{:S(2)}) collective-permute-start(bf16[128,256]{1,0:T(8,128)(2,1)S(1)} %copy-done.12), channel_id=1, source_target_pairs={{0,1},{1,2},{2,3},{3,4},{4,5},{5,6},{6,7},{7,0},{8,9},{9,10},{10,1... | collective-permute-start | bytes 196616 | tf_op jit(solution)/shard_map/ppermute | solution.py:206
  26.1 7.4 %collective-permute-start.4 = (bf16[128,256]{1,0:T(8,128)(2,1)S(1)}, bf16[128,256]{1,0:T(8,128)(2,1)S(1)}, u32[]{:S(2)}, u32[]{:S(2)}) collective-permute-start(bf16[128,256]{1,0:T(8,128)(2,1)S(1)} %copy-done.12), channel_id=1, source_target_pairs={{1,0},{2,1},{3,2},{4,3},{5,4},{6,5},{7,6},{0,7},{9,8},{10,9},{11,1... | collective-permute-start | bytes 196616 | tf_op jit(solution)/shard_map/ppermute | solution.py:211
  28.5 32.7 %copy-start.10 = (bf16[4,32,2,64]{1,3,0,2:T(8,128)(2,1)}, bf16[4,32,2,64]{1,3,0,2:T(8,128)(2,1)S(1)}, u32[]{:S(2)}) copy-start(bf16[4,32,2,64]{1,3,0,2:T(8,128)(2,1)S(1)} %copy.105) | copy-start | bytes 98308
  29.7 26.8 %copy-start.15 = (bf16[128,256]{1,0:T(8,128)(2,1)}, bf16[128,256]{1,0:T(8,128)(2,1)S(1)}, u32[]{:S(2)}) copy-start(bf16[128,256]{1,0:T(8,128)(2,1)S(1)} %collective-permute-done) | copy-start | bytes 196612
  29.7 3.7 %collective-permute-start.1 = (bf16[128,256]{1,0:T(8,128)(2,1)S(1)}, bf16[128,256]{1,0:T(8,128)(2,1)S(1)}, u32[]{:S(2)}, u32[]{:S(2)}) collective-permute-start(bf16[128,256]{1,0:T(8,128)(2,1)S(1)} %collective-permute-done), channel_id=1, source_target_pairs={{0,1},{1,2},{2,3},{3,4},{4,5},{5,6},{6,7},{7,0},{8,9},{9,10},{10,1... | collective-permute-start | bytes 196616 | tf_op jit(solution)/shard_map/ppermute | solution.py:206
  33.4 23.1 %copy-start.17 = (bf16[128,256]{1,0:T(8,128)(2,1)}, bf16[128,256]{1,0:T(8,128)(2,1)S(1)}, u32[]{:S(2)}) copy-start(bf16[128,256]{1,0:T(8,128)(2,1)S(1)} %collective-permute-done.1) | copy-start | bytes 196612
  33.4 3.7 %collective-permute-start.2 = (bf16[128,256]{1,0:T(8,128)(2,1)S(1)}, bf16[128,256]{1,0:T(8,128)(2,1)S(1)}, u32[]{:S(2)}, u32[]{:S(2)}) collective-permute-start(bf16[128,256]{1,0:T(8,128)(2,1)S(1)} %collective-permute-done.1), channel_id=1, source_target_pairs={{0,1},{1,2},{2,3},{3,4},{4,5},{5,6},{6,7},{7,0},{8,9},{9,10},{10,1... | collective-permute-start | bytes 196616 | tf_op jit(solution)/shard_map/ppermute | solution.py:206
  33.5 23.1 %copy-start.13 = (bf16[128,256]{1,0:T(8,128)(2,1)}, bf16[128,256]{1,0:T(8,128)(2,1)S(1)}, u32[]{:S(2)}) copy-start(bf16[128,256]{1,0:T(8,128)(2,1)S(1)} %collective-permute-done.4) | copy-start | bytes 196612
  33.5 4.3 %collective-permute-start.5 = (bf16[128,256]{1,0:T(8,128)(2,1)S(1)}, bf16[128,256]{1,0:T(8,128)(2,1)}, u32[]{:S(2)}, u32[]{:S(2)}) collective-permute-start(bf16[128,256]{1,0:T(8,128)(2,1)S(1)} %collective-permute-done.4), channel_id=1, source_target_pairs={{1,0},{2,1},{3,2},{4,3},{5,4},{6,5},{7,6},{0,7},{9,8},{10,9},{11,1... | collective-permute-start | bytes 196616 | tf_op jit(solution)/shard_map/ppermute | solution.py:211
  37.1 19.4 %copy-start.19 = (bf16[128,256]{1,0:T(8,128)(2,1)}, bf16[128,256]{1,0:T(8,128)(2,1)S(1)}, u32[]{:S(2)}) copy-start(bf16[128,256]{1,0:T(8,128)(2,1)S(1)} %collective-permute-done.2) | copy-start | bytes 196612
  37.1 3.7 %collective-permute-start.3 = (bf16[128,256]{1,0:T(8,128)(2,1)S(1)}, bf16[128,256]{1,0:T(8,128)(2,1)S(1)}, u32[]{:S(2)}, u32[]{:S(2)}) collective-permute-start(bf16[128,256]{1,0:T(8,128)(2,1)S(1)} %collective-permute-done.2), channel_id=1, source_target_pairs={{0,1},{1,2},{2,3},{3,4},{4,5},{5,6},{6,7},{7,0},{8,9},{9,10},{10,1... | collective-permute-start | bytes 196616 | tf_op jit(solution)/shard_map/ppermute | solution.py:206
  37.8 60.5 %collective-permute-start.6 = (bf16[128,256]{1,0:T(8,128)(2,1)}, bf16[128,256]{1,0:T(8,128)(2,1)}, u32[]{:S(2)}, u32[]{:S(2)}) collective-permute-start(bf16[128,256]{1,0:T(8,128)(2,1)} %collective-permute-done.5), channel_id=1, source_target_pairs={{1,0},{2,1},{3,2},{4,3},{5,4},{6,5},{7,6},{0,7},{9,8},{10,9},{11,1... | collective-permute-start | bytes 196616 | tf_op jit(solution)/shard_map/ppermute | solution.py:211
  60.8 1.2 copy-start.6
  61.5 0.8 copy-start.1
  61.6 0.7 copy-start.3
  65.4 8.0 %copy-start.20 = (bf16[128,256]{1,0:T(8,128)(2,1)S(1)}, bf16[128,256]{1,0:T(8,128)(2,1)}, u32[]{:S(2)}) copy-start(bf16[128,256]{1,0:T(8,128)(2,1)} %copy-done.19) | copy-start | bytes 196612
  65.5 8.7 %copy-start.18 = (bf16[128,256]{1,0:T(8,128)(2,1)S(1)}, bf16[128,256]{1,0:T(8,128)(2,1)}, u32[]{:S(2)}) copy-start(bf16[128,256]{1,0:T(8,128)(2,1)} %copy-done.17) | copy-start | bytes 196612
  65.5 9.2 %copy-start.16 = (bf16[128,256]{1,0:T(8,128)(2,1)S(1)}, bf16[128,256]{1,0:T(8,128)(2,1)}, u32[]{:S(2)}) copy-start(bf16[128,256]{1,0:T(8,128)(2,1)} %copy-done.15) | copy-start | bytes 196612
  65.5 10.5 %copy-start.2 = (f32[2,4,32,416]{3,2,1,0:T(8,128)S(1)}, f32[2,4,32,416]{3,2,1,0:T(8,128)}, u32[]{:S(2)}) copy-start(f32[2,4,32,416]{3,2,1,0:T(8,128)} %copy-done.1) | copy-start | bytes 1277956
  66.7 25.4 %all-to-all-start.1 = ((bf16[64,2,1,2048]{3,1,2,0:T(2,128)(2,1)}), bf16[64,2,1,2048]{3,1,2,0:T(2,128)(2,1)}, u32[]{:S(2)}, u32[]{:S(2)}) async-start(bf16[64,2,1,2048]{3,1,2,0:T(2,128)(2,1)} %bitcast.18), calls=%async_computation.1 | async-start | bytes 1048576 | tf_op jit(solution)/shard_map/all_to_all | solution.py:170
  76.4 1.0 copy-start
  80.4 17.0 %copy-start.5 = (bf16[8,128,256]{2,1,0:T(8,128)(2,1)S(1)}, bf16[8,128,256]{2,1,0:T(8,128)(2,1)}, u32[]{:S(2)}) copy-start(bf16[8,128,256]{2,1,0:T(8,128)(2,1)} %bitcast_dynamic-update-slice_fusion.3) | copy-start | bytes 1572868
  80.5 16.9 %copy-start.14 = (bf16[128,256]{1,0:T(8,128)(2,1)S(1)}, bf16[128,256]{1,0:T(8,128)(2,1)}, u32[]{:S(2)}) copy-start(bf16[128,256]{1,0:T(8,128)(2,1)} %copy-done.13) | copy-start | bytes 196612
  92.1 7.9 %copy-start.4 = (bf16[2,4,32,416]{3,2,1,0:T(8,128)(2,1)S(1)}, bf16[2,4,32,416]{3,2,1,0:T(8,128)(2,1)}, u32[]{:S(2)}) copy-start(bf16[2,4,32,416]{3,2,1,0:T(8,128)(2,1)} %copy-done.3) | copy-start | bytes 638980
  92.1 7.9 %copy-start.11 = (bf16[4,32,2,64]{1,3,0,2:T(8,128)(2,1)S(1)}, bf16[4,32,2,64]{1,3,0,2:T(8,128)(2,1)}, u32[]{:S(2)}) copy-start(bf16[4,32,2,64]{1,3,0,2:T(8,128)(2,1)} %copy-done.10) | copy-start | bytes 98308
  92.1 23.7 %all-to-all-start.2 = ((bf16[64,2,1,2048]{3,1,2,0:T(2,128)(2,1)}), bf16[64,2,1,2048]{3,1,2,0:T(2,128)(2,1)S(1)}, u32[]{:S(2)}, u32[]{:S(2)}) async-start(bf16[64,2,1,2048]{3,1,2,0:T(2,128)(2,1)} %bitcast.24), calls=%async_computation.2 | async-start | bytes 1048576 | tf_op jit(solution)/shard_map/all_to_all | solution.py:173
  101.5 20.7 %copy-start.9 = (bf16[128,128]{1,0:T(8,128)(2,1)}, bf16[128,128]{1,0:T(8,128)(2,1)S(1)}, u32[]{:S(2)}) copy-start(bf16[128,128]{1,0:T(8,128)(2,1)S(1)} %convert_element_type.81) | copy-start | bytes 98308
  115.8 23.3 %all-to-all-start.3 = ((bf16[64,32,128]{2,1,0:T(8,128)(2,1)}), bf16[64,32,128]{2,1,0:T(8,128)(2,1)S(1)}, u32[]{:S(2)}, u32[]{:S(2)}) async-start(bf16[64,32,128]{2,1,0:T(8,128)(2,1)} %bitcast.40), calls=%async_computation.3 | async-start | bytes 1048576 | tf_op jit(solution)/shard_map/all_to_all | solution.py:41
